TPU v7x, 32 devices: a whole 2x2x4 slice. The times are simulated.
32 devices in a mesh: sp: 8 (over z, x), tp: 4 (over y, core).
Axes of the slice: x: 2, y: 2, z: 4, core: 2. Of those that a mesh axis runs over, the one named last changes fastest.
Arguments:
- upstream: bfloat16 [2048, 2048], P('sp'), may hold values from -6 to 6
- stream: bfloat16 [2048, 2048], P('sp'), may hold values from -10 to 10
- routes: int32 [2048, 2], P('sp'), may hold values from 0 to 7, all different within a row; in each aligned block of 256 rows (0 to 255, 256 to 511, ...) at most 128 rows name the same one
- route_weights: float32 [2048, 2], P('sp'), may hold values from 0.1 to 1
- glu_value: bfloat16 [2048, 512], P('sp', 'tp'), may hold values from -6 to 6
- glu_gate: bfloat16 [2048, 512], P('sp', 'tp'), may hold values from -10 to 10
- conv_taps: float32 [31, 512], P(None, 'tp'), may hold values from -1 to 1
- conv_saved: bfloat16 [2048, 512], P('sp', 'tp'), may hold values from -600 to 600
- out_proj: bfloat16 [2048, 512], P(None, 'tp'), may hold values from -0.25 to 0.25
- expert_gate: bfloat16 [8, 2048, 2048], P('sp', None, 'tp'), may hold values from -0.125 to 0.125
- expert_up: bfloat16 [8, 2048, 2048], P('sp', None, 'tp'), may hold values from -0.125 to 0.125
- expert_down: bfloat16 [8, 2048, 2048], P('sp', 'tp'), may hold values from -0.125 to 0.125
Outputs:
- grad_stream: bfloat16 [2048, 2048], P('sp', 'tp')
- grad_value: bfloat16 [2048, 512], P('sp', 'tp')
- grad_gate: bfloat16 [2048, 512], P('sp', 'tp')
- grad_out_proj: float32 [2048, 512], P('sp', 'tp')
- grad_expert_gate: float32 [8, 2048, 2048], P('sp', None, 'tp')
- grad_expert_up: float32 [8, 2048, 2048], P('sp', None, 'tp')
- grad_expert_down: float32 [8, 2048, 2048], P('sp', 'tp')
Inputs may be any that keep to these rules, and one draw needn't show every extreme that they name: `routes`: each row names 2 different experts; among the 256 rows of one index of sp no expert is named more than 128 times, a bound that some block reaches.
All inputs are finite; a program needn't handle non-finite values.
Results may differ from a plain program's by a relative error of at most 0.014.
Values may be sent and summed in bfloat16 or wider, within the bound.
A program may use at most 128 MiB of HBM per device.

v0:
```python
import jax
import jax.numpy as jnp
from jax import lax
from jax.sharding import PartitionSpec as P

clamp_limit = 7.0
glu_alpha = 1.702
norm_eps = 1e-05


def passed_along(shard, axis, by):
    size = lax.axis_size(axis)
    pairs = [(i, i + by) for i in range(size) if 0 <= i + by < size]
    return lax.ppermute(shard, axis, pairs)


def contract_rows(left, right):
    return lax.dot_general(
        left, right, (((0,), (0,)), ((), ())), preferred_element_type=jnp.float32
    )


def times_transposed(left, right):
    return lax.dot_general(
        left, right, (((1,), (1,)), ((), ())), preferred_element_type=jnp.float32
    )


def pair_rows(block_routes, expert_count, capacity):
    tok_count, topk = block_routes.shape
    experts = jnp.arange(expert_count, dtype=jnp.int32)[None, :]
    hots = [(block_routes[:, k : k + 1] == experts).astype(jnp.float32) for k in range(topk)]
    before = (jnp.arange(tok_count)[:, None] > jnp.arange(tok_count)[None, :]).astype(jnp.bfloat16)
    earlier = jnp.dot(before, sum(hots).astype(jnp.bfloat16), preferred_element_type=jnp.float32)
    slots = [jnp.sum(earlier * hot, axis=1).astype(jnp.int32) for hot in hots]
    return [block_routes[:, k] * capacity + slots[k] for k in range(topk)]


def select_pairs(targets, block_weights, row_count):
    rows = jnp.arange(row_count, dtype=jnp.int32)[:, None]
    hits = [target[None, :] == rows for target in targets]
    picks = sum((hit.astype(jnp.float32) for hit in hits)).astype(jnp.bfloat16)
    row_weights = jnp.sum(
        sum((jnp.where(hit, block_weights[:, k][None, :], 0.0) for k, hit in enumerate(hits))),
        axis=1,
    )
    return (picks, row_weights)


def expert_backward(expert_rows, expert_cot, gate_weight, up_weight, down_weight):
    gate_pre = jnp.dot(expert_rows, gate_weight, preferred_element_type=jnp.float32)
    up_pre = jnp.dot(expert_rows, up_weight, preferred_element_type=jnp.float32)
    capped = jnp.minimum(gate_pre, clamp_limit)
    clipped = jnp.clip(up_pre, -clamp_limit, clamp_limit)
    gate_sigmoid = jax.nn.sigmoid(glu_alpha * capped)
    act = (capped * gate_sigmoid * (clipped + 1.0)).astype(jnp.bfloat16)
    grad_down = contract_rows(act, expert_cot)
    grad_act = times_transposed(expert_cot, down_weight)
    slope = gate_sigmoid + glu_alpha * capped * gate_sigmoid * (1.0 - gate_sigmoid)
    grad_gate_pre = jnp.where(
        gate_pre < clamp_limit, grad_act * (clipped + 1.0) * slope, 0.0
    ).astype(jnp.bfloat16)
    grad_up_pre = jnp.where(
        jnp.abs(up_pre) < clamp_limit, grad_act * capped * gate_sigmoid, 0.0
    ).astype(jnp.bfloat16)
    grad_gate = contract_rows(expert_rows, grad_gate_pre)
    grad_up = contract_rows(expert_rows, grad_up_pre)
    return (grad_gate, grad_up, grad_down, grad_gate_pre, grad_up_pre)


def on_device(
    upstream,
    stream,
    routes,
    route_weights,
    glu_value,
    glu_gate,
    conv_taps,
    conv_saved,
    out_proj,
    expert_gate,
    expert_up,
    expert_down,
):
    tok_count = upstream.shape[0]
    model_width = upstream.shape[1]
    expert_count = lax.axis_size("sp")
    capacity = 4 * tok_count // expert_count
    slice_width = model_width // lax.axis_size("tp")
    column_start = lax.axis_index("tp") * slice_width
    targets = pair_rows(routes, expert_count, capacity)
    picks, row_weights = select_pairs(targets, route_weights, expert_count * capacity)
    stream_part = lax.dynamic_slice_in_dim(stream, column_start, slice_width, 1)
    upstream_part = lax.dynamic_slice_in_dim(upstream, column_start, slice_width, 1)
    send_rows = jnp.dot(picks, stream_part, preferred_element_type=jnp.float32).astype(jnp.bfloat16)
    send_cot = (
        row_weights[:, None] * jnp.dot(picks, upstream_part, preferred_element_type=jnp.float32)
    ).astype(jnp.bfloat16)
    part_shape = (expert_count, capacity, slice_width)
    part_rows, part_cot = (
        lax.all_to_all(
            send_rows.reshape(part_shape), "sp", split_axis=0, concat_axis=0, tiled=True
        ),
        lax.all_to_all(send_cot.reshape(part_shape), "sp", split_axis=0, concat_axis=0, tiled=True),
    )
    got_rows, got_cot = (
        lax.all_gather(part_rows, "tp", axis=2, tiled=True),
        lax.all_gather(part_cot, "tp", axis=2, tiled=True),
    )
    expert_rows = got_rows.reshape(-1, model_width)
    expert_cot = got_cot.reshape(-1, model_width)
    gate_weight = expert_gate[0]
    up_weight = expert_up[0]
    down_weight = expert_down[0]
    grad_gate_w, grad_up_w, grad_down_w, grad_gate_pre, grad_up_pre = expert_backward(
        expert_rows, expert_cot, gate_weight, up_weight, down_weight
    )
    partial_rows = times_transposed(grad_gate_pre, gate_weight) + times_transposed(
        grad_up_pre, up_weight
    )
    summed_rows = lax.psum_scatter(
        partial_rows.astype(jnp.bfloat16), "tp", scatter_dimension=1, tiled=True
    )
    returned = lax.all_to_all(
        summed_rows.reshape(expert_count, capacity, slice_width),
        "sp",
        split_axis=0,
        concat_axis=0,
        tiled=True,
    )
    routed_sum = contract_rows(picks, returned.reshape(expert_count * capacity, slice_width))
    upstream_own = lax.dynamic_slice_in_dim(upstream, column_start, slice_width, 1)
    grad_stream = (upstream_own.astype(jnp.float32) + routed_sum).astype(jnp.bfloat16)
    full_grad = lax.all_gather(grad_stream, "tp", axis=1, tiled=True)
    conv_width = conv_saved.shape[1] * lax.axis_size("tp")
    saved_conv = conv_saved.astype(jnp.float32)
    total_sum, square_sum = lax.psum(
        (jnp.sum(saved_conv, axis=1), jnp.sum(saved_conv * saved_conv, axis=1)), "tp"
    )
    mean_c = (total_sum / conv_width)[:, None]
    var_c = (square_sum / conv_width)[:, None] - mean_c * mean_c
    inv_std = lax.rsqrt(var_c + norm_eps)
    normed = (saved_conv - mean_c) * inv_std
    norm_sigmoid = jax.nn.sigmoid(normed)
    mixed = (normed * norm_sigmoid).astype(jnp.bfloat16)
    grad_mixed = jnp.dot(full_grad, out_proj, preferred_element_type=jnp.float32)
    grad_normed = grad_mixed * norm_sigmoid * (1.0 + normed * (1.0 - norm_sigmoid))
    first_sum, second_sum = lax.psum(
        (jnp.sum(grad_normed, axis=1), jnp.sum(grad_normed * normed, axis=1)), "tp"
    )
    grad_conv = inv_std * (
        grad_normed
        - (first_sum / conv_width)[:, None]
        - normed * (second_sum / conv_width)[:, None]
    )
    kernel_width = conv_taps.shape[0]
    rim_rows = passed_along(grad_conv[: kernel_width - 1], "sp", -1)
    padded = jnp.concatenate([grad_conv, rim_rows], axis=0)
    grad_glu = jnp.zeros_like(grad_conv)
    for offset in range(kernel_width):
        grad_glu = grad_glu + conv_taps[offset][None, :] * padded[offset : offset + tok_count]
    gate_sig = jax.nn.sigmoid(glu_gate.astype(jnp.float32))
    grad_value = (grad_glu * gate_sig).astype(jnp.bfloat16)
    grad_gate = (grad_glu * glu_value.astype(jnp.float32) * gate_sig * (1.0 - gate_sig)).astype(
        jnp.bfloat16
    )
    proj_parts = contract_rows(full_grad, mixed).astype(jnp.bfloat16)
    proj_parts = lax.all_to_all(
        proj_parts.reshape(expert_count, -1, mixed.shape[1]),
        "sp",
        split_axis=0,
        concat_axis=0,
        tiled=True,
    )
    grad_out_proj = jnp.sum(proj_parts.astype(jnp.float32), axis=0)
    return (
        grad_stream,
        grad_value,
        grad_gate,
        grad_out_proj,
        grad_gate_w[None],
        grad_up_w[None],
        grad_down_w[None],
    )


def solution(mesh):
    in_specs = (
        P("sp", None),
        P("sp", None),
        P("sp", None),
        P("sp", None),
        P("sp", "tp"),
        P("sp", "tp"),
        P(None, "tp"),
        P("sp", "tp"),
        P(None, "tp"),
        P("sp", None, "tp"),
        P("sp", None, "tp"),
        P("sp", "tp", None),
    )
    out_specs = (
        P("sp", "tp"),
        P("sp", "tp"),
        P("sp", "tp"),
        P("sp", "tp"),
        P("sp", None, "tp"),
        P("sp", None, "tp"),
        P("sp", "tp", None),
    )
    return jax.shard_map(
        on_device, mesh=mesh, in_specs=in_specs, out_specs=out_specs, check_vma=False
    )
```

profile of v0, /device:TPU:0, one launch (start us, length us, event | category | flops | bytes accessed | tf_op | source)
XLA Modules:
  0.0 257.4 jit_solution(7277678649317412577)
XLA Ops:
  7.2 0.0 copy-start
  7.2 0.0 all-gather.4.cloned.1.call-start
  7.2 0.8 fusion.143
  8.1 0.2 select_reduce_fusion.1
  8.3 0.0 copy-start.5
  8.3 1.4 convolution_convert_fusion.1
  9.7 32.9 %all_to_all.20 = bf16[8,128,512]{2,1,0:T(8,128)(2,1)} all-to-all(bf16[8,128,512]{2,1,0:T(8,128)(2,1)S(1)} %bitcast.111), channel_id=1, replica_groups=mesh['sp'=8,'tp'=4] {'sp'}, dimensions={0} | all-to-all | bytes 2097152 | tf_op jit(solution)/shard_map/all_to_all | solution.py:101
  42.7 0.0 all-gather.4.cloned.1.call-update
  42.7 0.0 all-gather.6.cloned.1.call-start
  42.8 0.3 add_reduce_fusion
  43.1 1.4 multiply_convert_fusion.1
  44.5 29.0 %all_to_all.21 = bf16[8,128,512]{2,1,0:T(8,128)(2,1)} all-to-all(bf16[8,128,512]{2,1,0:T(8,128)(2,1)S(1)} %bitcast.110), channel_id=1, replica_groups=mesh['sp'=8,'tp'=4] {'sp'}, dimensions={0} | all-to-all | bytes 2097152 | tf_op jit(solution)/shard_map/all_to_all | solution.py:104
  73.4 0.0 all-gather.6.cloned.1.call-update
  73.5 0.0 reduce-scatter.2.cloned.1.call-start
  73.5 2.8 %all-gather.4.cloned.1.call-done = bf16[8,128,2048]{2,1,0:T(8,128)(2,1)} async-done(((bf16[8,128,512]{2,1,0:T(8,128)(2,1)}), bf16[8,128,2048]{2,1,0:T(8,128)(2,1)}) %all-gather.4.cloned.1.call-update) | async-done | bytes 4194320 | tf_op jit(solution)/shard_map/all_gather | solution.py:107
  76.3 6.6 %fusion.1 = f32[1024,512]{1,0:T(8,128)} fusion(bf16[1024,2048]{1,0:T(8,128)(2,1)} %bitcast.118, bf16[1,2048,512]{2,1,0:T(8,128)(2,1)} %param.22), kind=kOutput, calls=%fused_computation.6 | convolution fusion | flops 2147483648 | bytes 8388608 | tf_op jit(solution)/shard_map/dot_general | solution.py:52
  83.0 3.7 %fusion.7 = f32[1024,512]{1,0:T(8,128)} fusion(bf16[1024,2048]{1,0:T(8,128)(2,1)S(1)} %bitcast.121, bf16[1,2048,512]{2,1,0:T(8,128)(2,1)S(1)} %copy-done), kind=kOutput, calls=%fused_computation.12 | convolution fusion | flops 2147483648 | bytes 8388608 | tf_op jit(solution)/shard_map/dot_general | solution.py:51
  86.7 25.7 %all-gather.6.cloned.1.call-done = bf16[8,128,2048]{2,1,0:T(8,128)(2,1)} async-done(((bf16[8,128,512]{2,1,0:T(8,128)(2,1)}), bf16[8,128,2048]{2,1,0:T(8,128)(2,1)}) %all-gather.6.cloned.1.call-update) | async-done | bytes 4194320 | tf_op jit(solution)/shard_map/all_gather | solution.py:108
  112.4 7.6 %select_convert_fusion = (bf16[1024,512]{1,0:T(8,128)(2,1)S(1)}, bf16[1024,512]{1,0:T(8,128)(2,1)S(1)}) fusion(f32[1024,512]{1,0:T(8,128)} %fusion.1, f32[1024,512]{1,0:T(8,128)} %fusion.7, bf16[1024,2048]{1,0:T(8,128)(2,1)} %bitcast.122, bf16[1,512,2048]{2,1,0:T(8,128)(2,1)} %param.23), kind=kOutput, calls=%fused_computation.15 | convolution fusion | flops 2159017984 | bytes 12582912 | tf_op jit(solution)/shard_map/dot_general | solution.py:24
  120.0 0.0 copy-start.8
  120.1 2.4 fusion.5
  122.5 4.4 %add_convert_fusion = bf16[1024,2048]{1,0:T(8,128)(2,1)} fusion(f32[1024,2048]{1,0:T(8,128)S(1)} %fusion.5, bf16[1024,512]{1,0:T(8,128)(2,1)S(1)} %get-tuple-element.19, bf16[1,2048,512]{2,1,0:T(8,128)(2,1)S(1)} %copy-done.8), kind=kOutput, calls=%fused_computation | convolution fusion | flops 2151677952 | bytes 15728640 | tf_op jit(solution)/shard_map/dot_general | solution.py:24
  126.9 0.0 reduce-scatter.2.cloned.1.call-update
  126.9 0.0 copy-start.4
  126.9 44.5 %reduce-scatter.2.cloned.1.call-done = bf16[1024,512]{1,0:T(8,128)(2,1)} async-done(((bf16[1024,2048]{1,0:T(8,128)(2,1)}), bf16[1024,512]{1,0:T(8,128)(2,1)}) %reduce-scatter.2.cloned.1.call-update) | async-done | bytes 1048592 | tf_op jit(solution)/shard_map/reduce_scatter | solution.py:121
  171.4 5.7 %all-to-all-start.2 = ((bf16[8,128,512]{2,1,0:T(8,128)(2,1)}), bf16[8,128,512]{2,1,0:T(8,128)(2,1)S(1)}, u32[]{:S(2)}, u32[]{:S(2)}) async-start(bf16[8,128,512]{2,1,0:T(8,128)(2,1)} %bitcast.108), calls=%async_computation.3 | async-start | bytes 2097152 | tf_op jit(solution)/shard_map/all_to_all | solution.py:124
  177.1 0.0 all-gather.8.cloned.1.call-start
  177.2 0.1 fusion.112
  177.3 6.0 %all-reduce.1 = (f32[256]{0:T(256)S(1)}, f32[256]{0:T(256)S(1)}) all-reduce(f32[256]{0:T(256)S(1)} %get-tuple-element.10, f32[256]{0:T(256)S(1)} %get-tuple-element.9), channel_id=1, replica_groups=mesh['sp'=8,'tp'=4] {'tp'}, use_global_device_ids=true, to_apply=%region_7.8 | all-reduce | flops 512 | bytes 4096 | tf_op jit(solution)/shard_map/psum | solution.py:137
  183.3 19.5 %all-to-all-done.2 = bf16[8,128,512]{2,1,0:T(8,128)(2,1)S(1)} async-done(((bf16[8,128,512]{2,1,0:T(8,128)(2,1)}), bf16[8,128,512]{2,1,0:T(8,128)(2,1)S(1)}, u32[]{:S(2)}, u32[]{:S(2)}) %all-to-all-start.2) | async-done | bytes 1048608 | tf_op jit(solution)/shard_map/all_to_all | solution.py:124
  202.8 2.1 fusion.9
  204.9 0.0 all-gather.8.cloned.1.call-update
  205.0 7.0 %convolution_bitcast_fusion.1 = f32[1,2048,512]{2,1,0:T(8,128)} fusion(bf16[1024,2048]{1,0:T(8,128)(2,1)} %bitcast.119, bf16[1024,512]{1,0:T(8,128)(2,1)} %copy-done.10), kind=kOutput, calls=%fused_computation.2 | convolution fusion | flops 2147483648 | bytes 9437184 | tf_op jit(solution)/shard_map/dot_general | solution.py:18
  212.0 0.0 copy-start.9
  212.1 4.8 %convolution_bitcast_fusion = f32[1,512,2048]{2,1,0:T(8,128)} fusion(bf16[1024,2048]{1,0:T(8,128)(2,1)S(1)} %bitcast.123, f32[1024,512]{1,0:T(8,128)S(1)} %copy-done.13, f32[1024,512]{1,0:T(8,128)S(1)} %copy-done.12), kind=kOutput, calls=%fused_computation.1 | convolution fusion | flops 2152726528 | bytes 12582912 | tf_op jit(solution)/shard_map/dot_general | solution.py:18
  216.9 3.0 %all-gather.8.cloned.1.call-done = bf16[256,2048]{1,0:T(8,128)(2,1)} async-done(((bf16[256,512]{1,0:T(8,128)(2,1)}), bf16[256,2048]{1,0:T(8,128)(2,1)}) %all-gather.8.cloned.1.call-update) | async-done | bytes 1048592 | tf_op jit(solution)/shard_map/all_gather | solution.py:134
  219.8 1.8 fusion.141
  221.6 5.9 %all-reduce = (f32[256]{0:T(256)S(1)}, f32[256]{0:T(256)S(1)}) all-reduce(f32[256]{0:T(256)S(1)} %get-tuple-element.8, f32[256]{0:T(256)S(1)} %get-tuple-element.7), channel_id=1, replica_groups=mesh['sp'=8,'tp'=4] {'tp'}, use_global_device_ids=true, to_apply=%region_11.12 | all-reduce | flops 512 | bytes 4096 | tf_op jit(solution)/shard_map/psum | solution.py:148
  227.5 2.6 %convolution_convert_fusion = bf16[2048,128]{1,0:T(8,128)(2,1)} fusion(bf16[256,2048]{1,0:T(8,128)(2,1)} %all-gather.8.cloned.1.call-done, bf16[256,128]{1,0:T(8,128)(2,1)S(1)} %copy-done.2, f32[256]{0:T(256)S(1)} %get-tuple-element.57, f32[256]{0:T(256)S(1)} %get-tuple-element.56), kind=kOutput, calls=%fused_computation.4 | convolution fusion | flops 134742016 | bytes 1640448 | tf_op jit(solution)/shard_map/dot_general | solution.py:18
  230.1 5.7 %all-to-all-start.3 = ((bf16[8,256,128]{2,1,0:T(8,128)(2,1)}), bf16[8,256,128]{2,1,0:T(8,128)(2,1)S(1)}, u32[]{:S(2)}, u32[]{:S(2)}) async-start(bf16[8,256,128]{2,1,0:T(8,128)(2,1)} %bitcast.44), calls=%async_computation.4 | async-start | bytes 1048576 | tf_op jit(solution)/shard_map/all_to_all | solution.py:168
  235.8 0.2 fusion.125
  236.0 0.0 copy-start.1
  236.0 1.4 collective-permute-start
  237.4 6.9 %convolution_bitcast_fusion.2 = f32[1,2048,512]{2,1,0:T(8,128)} fusion(bf16[1024,2048]{1,0:T(8,128)(2,1)} %bitcast.120, bf16[1024,512]{1,0:T(8,128)(2,1)} %copy-done.11), kind=kOutput, calls=%fused_computation.3 | convolution fusion | flops 2147483648 | bytes 9437184 | tf_op jit(solution)/shard_map/dot_general | solution.py:18
  244.3 1.1 multiply_convert_fusion.3
  245.4 0.7 multiply_convert_fusion.4
  246.1 4.1 %all-to-all-done.3 = bf16[8,256,128]{2,1,0:T(8,128)(2,1)S(1)} async-done(((bf16[8,256,128]{2,1,0:T(8,128)(2,1)}), bf16[8,256,128]{2,1,0:T(8,128)(2,1)S(1)}, u32[]{:S(2)}, u32[]{:S(2)}) %all-to-all-start.3) | async-done | bytes 524320 | tf_op jit(solution)/shard_map/all_to_all | solution.py:168
  250.1 0.7 convert_reduce_fusion
  (31 shorter events, 0.1 us)
Async XLA Ops:
  7.2 75.8 %copy-start = (bf16[1,2048,512]{2,1,0:T(8,128)(2,1)S(1)}, bf16[1,2048,512]{2,1,0:T(8,128)(2,1)}, u32[]{:S(2)}) copy-start(bf16[1,2048,512]{2,1,0:T(8,128)(2,1)} %param.21) | copy-start | bytes 6291460
  7.2 69.2 %all-gather.4.cloned.1.call-start = ((), (), s32[]{:S(2)}) async-start(), calls=%async_computation.5 | async-start | bytes 5242880 | tf_op jit(solution)/shard_map/all_gather | solution.py:107
  8.3 34.5 %copy-start.5 = (f32[256,2]{0,1:T(2,128)S(1)}, f32[256,2]{0,1:T(2,128)}, u32[]{:S(2)}) copy-start(f32[256,2]{0,1:T(2,128)} %param.15) | copy-start | bytes 6148
  42.7 69.7 %all-gather.6.cloned.1.call-start = ((), (), s32[]{:S(2)}) async-start(), calls=%async_computation.6 | async-start | bytes 5242880 | tf_op jit(solution)/shard_map/all_gather | solution.py:108
  73.5 98.0 %reduce-scatter.2.cloned.1.call-start = ((), (), s32[]{:S(2)}) async-start(), calls=%async_computation.7 | async-start | bytes 5242880 | tf_op jit(solution)/shard_map/reduce_scatter | solution.py:121
  76.3 6.6 %copy-start.6 = (bf16[8,128,2048]{2,1,0:T(8,128)(2,1)S(1)}, bf16[8,128,2048]{2,1,0:T(8,128)(2,1)}, u32[]{:S(2)}) copy-start(bf16[8,128,2048]{2,1,0:T(8,128)(2,1)} %all-gather.4.cloned.1.call-done) | copy-start | bytes 12582916
  120.0 2.4 copy-start.11
  120.0 2.4 copy-start.10
  120.0 2.4 copy-start.8
  126.9 50.3 %copy-start.2 = (bf16[256,128]{1,0:T(8,128)(2,1)S(1)}, bf16[256,128]{1,0:T(8,128)(2,1)}, u32[]{:S(2)}) copy-start(bf16[256,128]{1,0:T(8,128)(2,1)} %param.19) | copy-start | bytes 196612
  126.9 56.4 %copy-start.4 = (f32[31,128]{1,0:T(8,128)S(1)}, f32[31,128]{1,0:T(8,128)}, u32[]{:S(2)}) copy-start(f32[31,128]{1,0:T(8,128)} %param.18) | copy-start | bytes 47620
  171.4 31.4 %all-to-all-start.2 = ((bf16[8,128,512]{2,1,0:T(8,128)(2,1)}), bf16[8,128,512]{2,1,0:T(8,128)(2,1)S(1)}, u32[]{:S(2)}, u32[]{:S(2)}) async-start(bf16[8,128,512]{2,1,0:T(8,128)(2,1)} %bitcast.108), calls=%async_computation.3 | async-start | bytes 2097152 | tf_op jit(solution)/shard_map/all_to_all | solution.py:124
  177.1 42.7 %all-gather.8.cloned.1.call-start = ((), (), s32[]{:S(2)}) async-start(), calls=%async_computation.8 | async-start | bytes 1310720 | tf_op jit(solution)/shard_map/all_gather | solution.py:134
  205.0 7.1 %copy-start.7 = (bf16[8,128,2048]{2,1,0:T(8,128)(2,1)S(1)}, bf16[8,128,2048]{2,1,0:T(8,128)(2,1)}, u32[]{:S(2)}) copy-start(bf16[8,128,2048]{2,1,0:T(8,128)(2,1)} %all-gather.6.cloned.1.call-done) | copy-start | bytes 12582916
  205.0 7.1 %copy-start.12 = (f32[1024,512]{1,0:T(8,128)S(1)}, f32[1024,512]{1,0:T(8,128)}, u32[]{:S(2)}) copy-start(f32[1024,512]{1,0:T(8,128)} %fusion.1) | copy-start | bytes 6291460
  205.0 7.0 %copy-start.13 = (f32[1024,512]{1,0:T(8,128)S(1)}, f32[1024,512]{1,0:T(8,128)}, u32[]{:S(2)}) copy-start(f32[1024,512]{1,0:T(8,128)} %fusion.7) | copy-start | bytes 6291460
  212.0 7.8 %copy-start.9 = (bf16[2048,128]{1,0:T(8,128)(2,1)S(1)}, bf16[2048,128]{1,0:T(8,128)(2,1)}, u32[]{:S(2)}) copy-start(bf16[2048,128]{1,0:T(8,128)(2,1)} %param.20) | copy-start | bytes 1572868
  230.1 20.0 %all-to-all-start.3 = ((bf16[8,256,128]{2,1,0:T(8,128)(2,1)}), bf16[8,256,128]{2,1,0:T(8,128)(2,1)S(1)}, u32[]{:S(2)}, u32[]{:S(2)}) async-start(bf16[8,256,128]{2,1,0:T(8,128)(2,1)} %bitcast.44), calls=%async_computation.4 | async-start | bytes 1048576 | tf_op jit(solution)/shard_map/all_to_all | solution.py:168
  236.0 8.3 %copy-start.1 = (bf16[256,128]{1,0:T(8,128)(2,1)S(1)}, bf16[256,128]{1,0:T(8,128)(2,1)}, u32[]{:S(2)}) copy-start(bf16[256,128]{1,0:T(8,128)(2,1)} %param.17) | copy-start | bytes 196612
  236.0 8.3 %copy-start.3 = (bf16[256,128]{1,0:T(8,128)(2,1)S(1)}, bf16[256,128]{1,0:T(8,128)(2,1)}, u32[]{:S(2)}) copy-start(bf16[256,128]{1,0:T(8,128)(2,1)} %param.16) | copy-start | bytes 196612
  236.0 8.3 %collective-permute-start = (f32[30,128]{1,0:T(8,128)S(1)}, f32[30,128]{1,0:T(8,128)S(1)}, u32[]{:S(2)}, u32[]{:S(2)}) collective-permute-start(f32[30,128]{1,0:T(8,128)S(1)} %slice.266), channel_id=1, source_target_pairs={{4,0},{8,4},{12,8},{16,12},{20,16},{24,20},{28,24},{5,1},{9,5},{13... | collective-permute-start | bytes 46088 | tf_op jit(solution)/shard_map/ppermute | solution.py:14
Sparse Core Ops, SparseCore 0:
  42.8 33.4 all-gather.3
  77.9 34.4 all-gather.5
  127.0 44.3 reduce-scatter.1
  205.1 14.7 all-gather.7
where the time goes:
time: 258 us; the launch traced here: 257 us
  waiting for transfers between devices  99.6 us (39%)
  blocking collectives  73.8 us (29%)
  matrix products  53 us (21%)
  between operations  14 us (5%)
  starting transfers between devices  12.9 us (5%)
  other arithmetic  3.14 us (1%)
    reduce_scatter x1, waiting for transfers between devices, on_device(): lax.psum_scatter(partial_rows.astype(jnp.bfloat16), 'tp', scatter_dimensi...  44.5 us
    all_to_all x1, blocking collectives, on_device(): lax.all_to_all(send_rows.reshape(part_shape), 'sp', split_axis=0, concat_...  32.9 us
    all_to_all x1, blocking collectives, on_device(): lax.all_to_all(send_cot.reshape(part_shape), 'sp', split_axis=0, concat_a...  29 us
    all_gather x1, waiting for transfers between devices, on_device(): lax.all_gather(part_cot, 'tp', axis=2, tiled=True)  25.7 us
    dot_general x5, matrix products, contract_rows(): lax.dot_general(left, right, (((0,), (0,)), ((), ())), preferred_element_...  23.4 us
    all_to_all x1, waiting for transfers between devices, on_device(): lax.all_to_all(summed_rows.reshape(expert_count, capacity, slice_width),...  19.5 us
    dot_general x3, matrix products, times_transposed(): lax.dot_general(left, right, (((1,), (1,)), ((), ())), preferred_element_...  14.4 us
    dot_general x1, matrix products, expert_backward(): up_pre = jnp.dot(expert_rows, up_weight, preferred_element_type=jnp.float32)  6.64 us
  transfers between devices with their start and end apart: 7, of which 6 were waited for; matrix products, arithmetic and copies ran while one was open for 13% of the time, Pallas kernels for 0%

commit v1 on v0

--- a/solution.py
+++ b/solution.py
@@ -6,6 +6,13 @@
 clamp_limit = 7.0
 glu_alpha = 1.702
 norm_eps = 1e-05
+
+
+def gather_over(x, axis, dim):
+    n_dev = lax.axis_size(axis)
+    parts = jnp.stack([x for _ in range(n_dev)])
+    parts = lax.all_to_all(parts, axis, split_axis=0, concat_axis=0)
+    return jnp.concatenate(parts, axis=dim)
 
 
 def passed_along(shard, axis, by):
@@ -105,7 +112,7 @@
     )
     got_rows, got_cot = (
         lax.all_gather(part_rows, "tp", axis=2, tiled=True),
-        lax.all_gather(part_cot, "tp", axis=2, tiled=True),
+        gather_over(part_cot, "tp", 2),
     )
     expert_rows = got_rows.reshape(-1, model_width)
     expert_cot = got_cot.reshape(-1, model_width)

time: 258 us -> 274 us (1.062)
  starting transfers between devices: 12.9 us -> 17.7 us
  waiting for transfers between devices: 99.6 us -> 104 us
  local copies, waits for them, and re-layouts: 0.95 us -> 5.21 us
    all_to_all x0 -> x1, waiting for transfers between devices: none -> 37.6 us  [gather_over(): parts = lax.all_to_all(parts, axis, split_axis=0, concat_axis=0)]
    all_gather x1 -> x0, waiting for transfers between devices: 25.7 us -> none  [on_device(): lax.all_gather(part_cot, 'tp', axis=2, tiled=True)]
    all_to_all x0 -> x1, starting transfers between devices: none -> 4.83 us  [gather_over(): parts = lax.all_to_all(parts, axis, split_axis=0, concat_axis=0)]
    all_gather x1, waiting for transfers between devices: 2.83 us -> 0.02 us  [on_device(): lax.all_gather(part_rows, 'tp', axis=2, tiled=True)]
  transfers between devices with their start and end apart: 7 -> 7, of which waited for: 6 -> 5; matrix products, arithmetic and copies ran while one was open for 13% -> 14% of each run, Pallas kernels for 0% -> 0%
where the time goes in v1:
time: 274 us
  waiting for transfers between devices  104 us (38%)
  blocking collectives  74 us (27%)
  matrix products  55.6 us (20%)
  starting transfers between devices  17.7 us (6%)
  between operations  14 us (5%)
  local copies, waits for them, and re-layouts  5.21 us (2%)
  other arithmetic  3.14 us (1%)
    reduce_scatter x1, waiting for transfers between devices, on_device(): lax.psum_scatter(partial_rows.astype(jnp.bfloat16), 'tp', scatter_dimensi...  42.6 us
    all_to_all x1, waiting for transfers between devices, gather_over(): parts = lax.all_to_all(parts, axis, split_axis=0, concat_axis=0)  37.6 us
    all_to_all x1, blocking collectives, on_device(): lax.all_to_all(send_rows.reshape(part_shape), 'sp', split_axis=0, concat_...  32.9 us
    all_to_all x1, blocking collectives, on_device(): lax.all_to_all(send_cot.reshape(part_shape), 'sp', split_axis=0, concat_a...  29 us
    dot_general x5, matrix products, contract_rows(): lax.dot_general(left, right, (((0,), (0,)), ((), ())), preferred_element_...  26 us
    all_to_all x1, waiting for transfers between devices, on_device(): lax.all_to_all(summed_rows.reshape(expert_count, capacity, slice_width),...  19.2 us
    dot_general x3, matrix products, times_transposed(): lax.dot_general(left, right, (((1,), (1,)), ((), ())), preferred_element_...  14.5 us
    dot_general x1, matrix products, expert_backward(): up_pre = jnp.dot(expert_rows, up_weight, preferred_element_type=jnp.float32)  6.65 us
  transfers between devices with their start and end apart: 7, of which 5 were waited for; matrix products, arithmetic and copies ran while one was open for 14% of the time, Pallas kernels for 0%

profile of v1, /device:TPU:0, one launch (start us, length us, event | category | flops | bytes accessed | tf_op | source)
XLA Modules:
  0.0 273.7 jit_solution(3366596403971953291)
XLA Ops:
  7.2 0.0 copy-start
  7.2 0.0 all-gather.3.cloned.1.call-start
  7.2 0.8 fusion.151
  8.1 0.2 select_reduce_fusion.1
  8.3 0.0 copy-start.5
  8.3 1.4 convolution_convert_fusion.1
  9.7 32.9 %all_to_all.25 = bf16[8,128,512]{2,1,0:T(8,128)(2,1)} all-to-all(bf16[8,128,512]{2,1,0:T(8,128)(2,1)S(1)} %bitcast.122), channel_id=1, replica_groups=mesh['sp'=8,'tp'=4] {'sp'}, dimensions={0} | all-to-all | bytes 2097152 | tf_op jit(solution)/shard_map/all_to_all | solution.py:108
  42.7 0.0 all-gather.3.cloned.1.call-update
  42.7 0.3 add_reduce_fusion
  43.0 1.4 multiply_convert_fusion.1
  44.4 29.0 %all_to_all.26 = bf16[8,128,512]{2,1,0:T(8,128)(2,1)} all-to-all(bf16[8,128,512]{2,1,0:T(8,128)(2,1)S(1)} %bitcast.121), channel_id=1, replica_groups=mesh['sp'=8,'tp'=4] {'sp'}, dimensions={0} | all-to-all | bytes 2097152 | tf_op jit(solution)/shard_map/all_to_all | solution.py:111
  73.4 1.7 copy.20
  75.1 2.6 stack.2
  77.7 4.8 %all-to-all-start.2 = ((bf16[4,8,128,512]{2,1,3,0:T(8,128)(2,1)}), bf16[4,8,128,512]{2,1,3,0:T(8,128)(2,1)}, u32[]{:S(2)}, u32[]{:S(2)}) async-start(bf16[4,8,128,512]{2,1,3,0:T(8,128)(2,1)} %stack.2), calls=%async_computation.2 | async-start | bytes 8388608 | tf_op jit(solution)/shard_map/all_to_all | solution.py:14
  82.5 0.2 reduce-scatter.2.cloned.1.call-start
  82.7 0.0 all-gather.3.cloned.1.call-done
  82.8 6.6 %fusion.10 = f32[1024,512]{1,0:T(8,128)} fusion(bf16[1024,2048]{1,0:T(8,128)(2,1)} %bitcast.129, bf16[1,2048,512]{2,1,0:T(8,128)(2,1)} %param.22), kind=kOutput, calls=%fused_computation.12 | convolution fusion | flops 2147483648 | bytes 8388608 | tf_op jit(solution)/shard_map/dot_general | solution.py:59
  89.4 3.7 %fusion.15 = f32[1024,512]{1,0:T(8,128)} fusion(bf16[1024,2048]{1,0:T(8,128)(2,1)S(1)} %bitcast.132, bf16[1,2048,512]{2,1,0:T(8,128)(2,1)S(1)} %copy-done), kind=kOutput, calls=%fused_computation.17 | convolution fusion | flops 2147483648 | bytes 8388608 | tf_op jit(solution)/shard_map/dot_general | solution.py:58
  93.1 37.6 %all-to-all-done.2 = bf16[4,8,128,512]{2,1,3,0:T(8,128)(2,1)} async-done(((bf16[4,8,128,512]{2,1,3,0:T(8,128)(2,1)}), bf16[4,8,128,512]{2,1,3,0:T(8,128)(2,1)}, u32[]{:S(2)}, u32[]{:S(2)}) %all-to-all-start.2) | async-done | bytes 4194336 | tf_op jit(solution)/shard_map/all_to_all | solution.py:14
  130.7 7.7 %select_convert_fusion = (bf16[1024,512]{1,0:T(8,128)(2,1)S(1)}, bf16[1024,512]{1,0:T(8,128)(2,1)S(1)}) fusion(f32[1024,512]{1,0:T(8,128)} %fusion.10, f32[1024,512]{1,0:T(8,128)} %fusion.15, bf16[1,512,2048]{2,1,0:T(8,128)(2,1)} %param.23, bf16[256,8,8,128]{3,2,1,0:T(8,128)(2,1)} %bitcast.50), kind=kOutput, calls=%fused_computation.20 | convolution fusion | flops 2159017984 | bytes 12582912 | tf_op jit(solution)/shard_map/dot_general | solution.py:31
  138.4 0.0 copy-start.7
  138.5 2.4 fusion.13
  140.9 4.4 %add_convert_fusion = bf16[1024,2048]{1,0:T(8,128)(2,1)} fusion(f32[1024,2048]{1,0:T(8,128)S(1)} %fusion.13, bf16[1024,512]{1,0:T(8,128)(2,1)S(1)} %get-tuple-element.19, bf16[1,2048,512]{2,1,0:T(8,128)(2,1)S(1)} %copy-done.7), kind=kOutput, calls=%fused_computation | convolution fusion | flops 2151677952 | bytes 15728640 | tf_op jit(solution)/shard_map/dot_general | solution.py:31
  145.2 0.0 reduce-scatter.2.cloned.1.call-update
  145.3 0.0 copy-start.4
  145.3 42.6 %reduce-scatter.2.cloned.1.call-done = bf16[1024,512]{1,0:T(8,128)(2,1)} async-done(((bf16[1024,2048]{1,0:T(8,128)(2,1)}), bf16[1024,512]{1,0:T(8,128)(2,1)}) %reduce-scatter.2.cloned.1.call-update) | async-done | bytes 1048592 | tf_op jit(solution)/shard_map/reduce_scatter | solution.py:128
  187.9 5.5 %all-to-all-start.3 = ((bf16[8,128,512]{2,1,0:T(8,128)(2,1)}), bf16[8,128,512]{2,1,0:T(8,128)(2,1)S(1)}, u32[]{:S(2)}, u32[]{:S(2)}) async-start(bf16[8,128,512]{2,1,0:T(8,128)(2,1)} %bitcast.119), calls=%async_computation.4 | async-start | bytes 2097152 | tf_op jit(solution)/shard_map/all_to_all | solution.py:131
  193.4 0.0 all-gather.5.cloned.1.call-start
  193.4 0.1 fusion.120
  193.6 6.2 %all-reduce.1 = (f32[256]{0:T(256)S(1)}, f32[256]{0:T(256)S(1)}) all-reduce(f32[256]{0:T(256)S(1)} %get-tuple-element.10, f32[256]{0:T(256)S(1)} %get-tuple-element.9), channel_id=1, replica_groups=mesh['sp'=8,'tp'=4] {'tp'}, use_global_device_ids=true, to_apply=%region_7.8 | all-reduce | flops 512 | bytes 4096 | tf_op jit(solution)/shard_map/psum | solution.py:144
  199.8 19.2 %all-to-all-done.3 = bf16[8,128,512]{2,1,0:T(8,128)(2,1)S(1)} async-done(((bf16[8,128,512]{2,1,0:T(8,128)(2,1)}), bf16[8,128,512]{2,1,0:T(8,128)(2,1)S(1)}, u32[]{:S(2)}, u32[]{:S(2)}) %all-to-all-start.3) | async-done | bytes 1048608 | tf_op jit(solution)/shard_map/all_to_all | solution.py:131
  219.0 2.1 fusion.17
  221.2 0.0 all-gather.5.cloned.1.call-update
  221.2 7.0 %convolution_bitcast_fusion = f32[1,2048,512]{2,1,0:T(8,128)} fusion(bf16[1024,2048]{1,0:T(8,128)(2,1)} %bitcast.130, bf16[1024,512]{1,0:T(8,128)(2,1)} %copy-done.9), kind=kOutput, calls=%fused_computation.8 | convolution fusion | flops 2147483648 | bytes 9437184 | tf_op jit(solution)/shard_map/dot_general | solution.py:25
  228.3 7.3 %fusion.6 = f32[1,512,2048]{2,1,0:T(8,128)} fusion(bf16[256,8,8,128]{3,2,1,0:T(8,128)(2,1)} %bitcast.50, f32[1024,512]{1,0:T(8,128)S(1)} %copy-done.12, f32[1024,512]{1,0:T(8,128)S(1)} %copy-done.11), kind=kOutput, calls=%fused_computation.7 | convolution fusion | flops 2152726528 | bytes 12582912 | tf_op jit(solution)/shard_map/dot_general | solution.py:25
  235.6 0.5 all-gather.5.cloned.1.call-done
  236.1 1.8 fusion.149
  237.9 5.9 %all-reduce = (f32[256]{0:T(256)S(1)}, f32[256]{0:T(256)S(1)}) all-reduce(f32[256]{0:T(256)S(1)} %get-tuple-element.8, f32[256]{0:T(256)S(1)} %get-tuple-element.7), channel_id=1, replica_groups=mesh['sp'=8,'tp'=4] {'tp'}, use_global_device_ids=true, to_apply=%region_11.12 | all-reduce | flops 512 | bytes 4096 | tf_op jit(solution)/shard_map/psum | solution.py:155
  243.8 2.6 convolution_convert_fusion
  246.4 5.7 %all-to-all-start.4 = ((bf16[8,256,128]{2,1,0:T(8,128)(2,1)}), bf16[8,256,128]{2,1,0:T(8,128)(2,1)S(1)}, u32[]{:S(2)}, u32[]{:S(2)}) async-start(bf16[8,256,128]{2,1,0:T(8,128)(2,1)} %bitcast.44), calls=%async_computation.5 | async-start | bytes 1048576 | tf_op jit(solution)/shard_map/all_to_all | solution.py:175
  252.0 0.2 fusion.133
  252.3 0.0 copy-start.1
  252.3 1.4 collective-permute-start
  253.7 6.9 %convolution_bitcast_fusion.1 = f32[1,2048,512]{2,1,0:T(8,128)} fusion(bf16[1024,2048]{1,0:T(8,128)(2,1)} %bitcast.131, bf16[1024,512]{1,0:T(8,128)(2,1)} %copy-done.10), kind=kOutput, calls=%fused_computation.9 | convolution fusion | flops 2147483648 | bytes 9437184 | tf_op jit(solution)/shard_map/dot_general | solution.py:25
  260.6 1.1 multiply_convert_fusion.3
  261.7 0.7 multiply_convert_fusion.4
  262.3 4.1 %all-to-all-done.4 = bf16[8,256,128]{2,1,0:T(8,128)(2,1)S(1)} async-done(((bf16[8,256,128]{2,1,0:T(8,128)(2,1)}), bf16[8,256,128]{2,1,0:T(8,128)(2,1)S(1)}, u32[]{:S(2)}, u32[]{:S(2)}) %all-to-all-start.4) | async-done | bytes 524320 | tf_op jit(solution)/shard_map/all_to_all | solution.py:175
  266.4 0.7 convert_reduce_fusion
  (30 shorter events, 0.1 us)
Async XLA Ops:
  7.2 82.2 %copy-start = (bf16[1,2048,512]{2,1,0:T(8,128)(2,1)S(1)}, bf16[1,2048,512]{2,1,0:T(8,128)(2,1)}, u32[]{:S(2)}) copy-start(bf16[1,2048,512]{2,1,0:T(8,128)(2,1)} %param.21) | copy-start | bytes 6291460
  7.2 75.6 %all-gather.3.cloned.1.call-start = ((), (), s32[]{:S(2)}) async-start(), calls=%async_computation.6 | async-start | bytes 5242880 | tf_op jit(solution)/shard_map/all_gather | solution.py:114
  8.3 34.4 %copy-start.5 = (f32[256,2]{0,1:T(2,128)S(1)}, f32[256,2]{0,1:T(2,128)}, u32[]{:S(2)}) copy-start(f32[256,2]{0,1:T(2,128)} %param.15) | copy-start | bytes 6148
  77.7 53.0 %all-to-all-start.2 = ((bf16[4,8,128,512]{2,1,3,0:T(8,128)(2,1)}), bf16[4,8,128,512]{2,1,3,0:T(8,128)(2,1)}, u32[]{:S(2)}, u32[]{:S(2)}) async-start(bf16[4,8,128,512]{2,1,3,0:T(8,128)(2,1)} %stack.2), calls=%async_computation.2 | async-start | bytes 8388608 | tf_op jit(solution)/shard_map/all_to_all | solution.py:14
  82.5 105.4 %reduce-scatter.2.cloned.1.call-start = ((), (), s32[]{:S(2)}) async-start(), calls=%async_computation.7 | async-start | bytes 5242880 | tf_op jit(solution)/shard_map/reduce_scatter | solution.py:128
  82.7 6.7 %copy-start.6 = (bf16[8,128,2048]{2,1,0:T(8,128)(2,1)S(1)}, bf16[8,128,2048]{2,1,0:T(8,128)(2,1)}, u32[]{:S(2)}) copy-start(bf16[8,128,2048]{2,1,0:T(8,128)(2,1)} %all-gather.3.cloned.1.call-done) | copy-start | bytes 12582916
  138.4 2.4 copy-start.10
  138.4 2.4 copy-start.9
  138.4 2.4 copy-start.7
  145.3 48.2 %copy-start.2 = (bf16[256,128]{1,0:T(8,128)(2,1)S(1)}, bf16[256,128]{1,0:T(8,128)(2,1)}, u32[]{:S(2)}) copy-start(bf16[256,128]{1,0:T(8,128)(2,1)} %param.19) | copy-start | bytes 196612
  145.3 54.5 %copy-start.4 = (f32[31,128]{1,0:T(8,128)S(1)}, f32[31,128]{1,0:T(8,128)}, u32[]{:S(2)}) copy-start(f32[31,128]{1,0:T(8,128)} %param.18) | copy-start | bytes 47620
  187.9 31.2 %all-to-all-start.3 = ((bf16[8,128,512]{2,1,0:T(8,128)(2,1)}), bf16[8,128,512]{2,1,0:T(8,128)(2,1)S(1)}, u32[]{:S(2)}, u32[]{:S(2)}) async-start(bf16[8,128,512]{2,1,0:T(8,128)(2,1)} %bitcast.119), calls=%async_computation.4 | async-start | bytes 2097152 | tf_op jit(solution)/shard_map/all_to_all | solution.py:131
  193.4 42.7 %all-gather.5.cloned.1.call-start = ((), (), s32[]{:S(2)}) async-start(), calls=%async_computation.8 | async-start | bytes 1310720 | tf_op jit(solution)/shard_map/all_gather | solution.py:141
  221.2 7.1 %copy-start.11 = (f32[1024,512]{1,0:T(8,128)S(1)}, f32[1024,512]{1,0:T(8,128)}, u32[]{:S(2)}) copy-start(f32[1024,512]{1,0:T(8,128)} %fusion.10) | copy-start | bytes 6291460
  221.2 7.0 %copy-start.12 = (f32[1024,512]{1,0:T(8,128)S(1)}, f32[1024,512]{1,0:T(8,128)}, u32[]{:S(2)}) copy-start(f32[1024,512]{1,0:T(8,128)} %fusion.15) | copy-start | bytes 6291460
  228.3 7.8 %copy-start.8 = (bf16[2048,128]{1,0:T(8,128)(2,1)S(1)}, bf16[2048,128]{1,0:T(8,128)(2,1)}, u32[]{:S(2)}) copy-start(bf16[2048,128]{1,0:T(8,128)(2,1)} %param.20) | copy-start | bytes 1572868
  246.4 20.0 %all-to-all-start.4 = ((bf16[8,256,128]{2,1,0:T(8,128)(2,1)}), bf16[8,256,128]{2,1,0:T(8,128)(2,1)S(1)}, u32[]{:S(2)}, u32[]{:S(2)}) async-start(bf16[8,256,128]{2,1,0:T(8,128)(2,1)} %bitcast.44), calls=%async_computation.5 | async-start | bytes 1048576 | tf_op jit(solution)/shard_map/all_to_all | solution.py:175
  252.3 8.3 %copy-start.1 = (bf16[256,128]{1,0:T(8,128)(2,1)S(1)}, bf16[256,128]{1,0:T(8,128)(2,1)}, u32[]{:S(2)}) copy-start(bf16[256,128]{1,0:T(8,128)(2,1)} %param.17) | copy-start | bytes 196612
  252.3 8.3 %copy-start.3 = (bf16[256,128]{1,0:T(8,128)(2,1)S(1)}, bf16[256,128]{1,0:T(8,128)(2,1)}, u32[]{:S(2)}) copy-start(bf16[256,128]{1,0:T(8,128)(2,1)} %param.16) | copy-start | bytes 196612
  252.3 8.3 %collective-permute-start = (f32[30,128]{1,0:T(8,128)S(1)}, f32[30,128]{1,0:T(8,128)S(1)}, u32[]{:S(2)}, u32[]{:S(2)}) collective-permute-start(f32[30,128]{1,0:T(8,128)S(1)} %slice.266), channel_id=1, source_target_pairs={{4,0},{8,4},{12,8},{16,12},{20,16},{24,20},{28,24},{5,1},{9,5},{13... | collective-permute-start | bytes 46088 | tf_op jit(solution)/shard_map/ppermute | solution.py:21
Sparse Core Ops, SparseCore 0:
  42.8 33.4 all-gather.2
  145.4 42.4 reduce-scatter.1
  221.3 14.7 all-gather.4
